TPU v7x, 32 devices: a whole 2x2x4 slice. The times are simulated.
32 devices in a mesh: fs: 16 (over z, y, x), tp: 2 (over core).
Axes of the slice: x: 2, y: 2, z: 4, core: 2. Of those that a mesh axis runs over, the one named last changes fastest.
Arguments:
- fwd_input: bfloat16 [2048, 2048], P('fs'), may hold values from -6 to 6
- saved_input: bfloat16 [2048, 2048], P('fs'), may hold values from -6 to 6
- out_cotangent: bfloat16 [2048, 2048], P('fs'), may hold values from -6 to 6
- up_weight: bfloat16 [2048, 4096], P('fs', 'tp'), may hold values from -0.125 to 0.125
- down_weight: bfloat16 [4096, 2048], P('tp', 'fs'), may hold values from -0.09375 to 0.09375
- up_grad_sum: float32 [2048, 4096], P('fs', 'tp'), may hold values from -6 to 6
Outputs:
- layer_out: bfloat16 [2048, 2048], P('fs')
- input_grad: bfloat16 [2048, 2048], P('fs')
- up_grad_out: float32 [2048, 4096], P('fs', 'tp')
All inputs are finite; a program needn't handle non-finite values.
Results may differ from a plain program's by a relative error of at most 0.013.
Values may be sent and summed in bfloat16 or wider, within the bound.
A program may use at most 128 MiB of HBM per device.

v0:
```python
import jax
import jax.numpy as jnp
from jax import lax
from jax.sharding import PartitionSpec as P


def per_device(fwd_input, saved_input, out_cotangent, up_weight, down_weight, up_grad_sum):
    row_count = fwd_input.shape[0]
    stacked = jnp.concatenate([fwd_input, saved_input], axis=0)
    up_whole = lax.all_gather(up_weight, "fs", axis=0, tiled=True)
    down_whole = lax.all_gather(down_weight, "fs", axis=1, tiled=True)
    pre_both = jnp.dot(stacked, up_whole, preferred_element_type=jnp.float32)
    pre_fwd = pre_both[:row_count]
    pre_bwd = pre_both[row_count:]
    positive = jnp.maximum(pre_fwd, 0.0)
    hidden = (positive * positive).astype(jnp.bfloat16)
    out_part = jnp.dot(hidden, down_whole, preferred_element_type=jnp.float32)
    layer_out = lax.psum(out_part.astype(jnp.bfloat16), "tp")
    d_hidden = lax.dot_general(
        out_cotangent, down_whole, (((1,), (1,)), ((), ())), preferred_element_type=jnp.float32
    )
    d_pre = (d_hidden * 2.0 * jnp.maximum(pre_bwd, 0.0)).astype(jnp.bfloat16)
    in_part = lax.dot_general(
        d_pre, up_whole, (((1,), (1,)), ((), ())), preferred_element_type=jnp.float32
    )
    input_grad = lax.psum(in_part.astype(jnp.bfloat16), "tp")
    grad_part = lax.psum_scatter(
        lax.dot_general(
            saved_input, d_pre, (((0,), (0,)), ((), ())), preferred_element_type=jnp.float32
        ),
        "fs",
        scatter_dimension=0,
        tiled=True,
    )
    grad_scale = float(row_count * lax.axis_size("fs")) ** (-0.5)
    return (layer_out, input_grad, up_grad_sum + grad_part * grad_scale)


def solution(mesh):
    placed = (
        P("fs", None),
        P("fs", None),
        P("fs", None),
        P("fs", "tp"),
        P("tp", "fs"),
        P("fs", "tp"),
    )
    return jax.shard_map(
        per_device,
        mesh=mesh,
        in_specs=placed,
        out_specs=(P("fs", None), P("fs", None), P("fs", "tp")),
        check_vma=False,
    )
```

profile of v0, /device:TPU:0, one launch (start us, length us, event | category | flops | bytes accessed | tf_op | source)
XLA Modules:
  0.0 666.1 jit_solution(1798604370416390500)
XLA Ops:
  7.2 0.0 copy-start
  7.2 0.0 all-gather.3.cloned.1.call-start
  7.2 0.7 all-gather.3.cloned.1.call-update
  7.9 0.0 all-gather.5.cloned.1.call-start
  8.0 0.7 all-gather.5.cloned.1.call-update
  8.7 0.0 reduce-scatter.2.cloned.1.call-start
  8.7 117.1 %all-gather.3.cloned.1.call-done = bf16[2048,2048]{1,0:T(8,128)(2,1)} async-done(((bf16[128,2048]{1,0:T(8,128)(2,1)}), bf16[2048,2048]{1,0:T(8,128)(2,1)}) %all-gather.3.cloned.1.call-update) | async-done | bytes 8388624 | tf_op jit(solution)/shard_map/all_gather | solution.py:10
  125.8 6.0 fusion.4
  131.9 136.7 %all-gather.5.cloned.1.call-done = bf16[2048,2048]{1,0:T(8,128)(2,1)} async-done(((bf16[2048,128]{1,0:T(8,128)(2,1)}), bf16[2048,2048]{1,0:T(8,128)(2,1)}) %all-gather.5.cloned.1.call-update) | async-done | bytes 8388624 | tf_op jit(solution)/shard_map/all_gather | solution.py:11
  268.6 0.0 copy-done
  268.6 0.0 copy-start.1
  268.6 6.3 fusion.1
  274.9 0.0 copy-done.1
  274.9 8.1 %convolution_bitcast_fusion = f32[2048,2048]{0,1:T(8,128)} fusion(bf16[128,2048]{1,0:T(8,128)(2,1)S(1)} %fusion.1, bf16[128,2048]{1,0:T(8,128)(2,1)S(1)} %copy-done.1), kind=kOutput, calls=%fused_computation | convolution fusion | flops 1073741824 | bytes 17825792 | tf_op jit(solution)/shard_map/dot_general | solution.py:28
  283.0 0.0 reduce-scatter.2.cloned.1.call-update
  283.0 0.0 all-reduce.3.cloned.1.call-start
  283.1 7.1 %convolution_convert_fusion = bf16[128,2048]{1,0:T(8,128)(2,1)} fusion(bf16[128,2048]{1,0:T(8,128)(2,1)S(1)} %fusion.1, bf16[2048,2048]{1,0:T(8,128)(2,1)} %all-gather.3.cloned.1.call-done), kind=kOutput, calls=%fused_computation.3 | convolution fusion | flops 1074003968 | bytes 9437184 | tf_op jit(solution)/shard_map/dot_general | solution.py:23
  290.2 5.4 convolution_convert_fusion.1
  295.6 0.0 all-reduce.3.cloned.1.call-update
  295.6 1.6 copy.9
  297.2 330.6 %reduce-scatter.2.cloned.1.call-done = f32[128,2048]{0,1:T(8,128)} async-done(((f32[2048,2048]{0,1:T(8,128)}), f32[128,2048]{0,1:T(8,128)}) %reduce-scatter.2.cloned.1.call-update) | async-done | bytes 1048592 | tf_op jit(solution)/shard_map/reduce_scatter | solution.py:27
  627.8 1.3 multiply_add_fusion
  629.2 1.3 copy.10
  630.5 25.3 %all-reduce.3.cloned.1.call-done = (bf16[128,2048]{1,0:T(8,128)(2,1)}, bf16[128,2048]{1,0:T(8,128)(2,1)}) async-done(((bf16[128,2048]{1,0:T(8,128)(2,1)}, bf16[128,2048]{1,0:T(8,128)(2,1)}), (bf16[128,2048]{1,0:T(8,128)(2,1)}, bf16[128,2048]{1,0:T(8,128)(2,1)})) %all-reduce.3.cloned.1.call-update) | async-done | bytes 1048592 | tf_op jit(solution)/shard_map/psum | solution.py:18
  655.8 1.9 copy.13
  657.7 1.9 copy.14
Async XLA Ops:
  7.2 261.4 %copy-start = (bf16[128,2048]{1,0:T(8,128)(2,1)S(1)}, bf16[128,2048]{1,0:T(8,128)(2,1)}, u32[]{:S(2)}) copy-start(bf16[128,2048]{1,0:T(8,128)(2,1)} %param.8) | copy-start | bytes 1572868
  7.2 118.6 %all-gather.3.cloned.1.call-start = ((), (), s32[]{:S(2)}) async-start(), calls=%async_computation.1 | async-start | bytes 8912896 | tf_op jit(solution)/shard_map/all_gather | solution.py:10
  7.9 260.6 %all-gather.5.cloned.1.call-start = ((), (), s32[]{:S(2)}) async-start(), calls=%async_computation.2 | async-start | bytes 8912896 | tf_op jit(solution)/shard_map/all_gather | solution.py:11
  8.7 619.1 %reduce-scatter.2.cloned.1.call-start = ((), (), s32[]{:S(2)}) async-start(), calls=%async_computation.3 | async-start | bytes 17825792 | tf_op jit(solution)/shard_map/reduce_scatter | solution.py:27
  268.6 6.3 copy-start.1
  283.0 372.7 %all-reduce.3.cloned.1.call-start = ((), (), s32[]{:S(2)}) async-start(), calls=%async_computation.4 | async-start | bytes 2097152 | tf_op jit(solution)/shard_map/psum | solution.py:18
Sparse Core Ops, SparseCore 0:
  10.8 115.0 all-gather.2
  128.5 139.9 all-gather.4
  283.2 344.5 reduce-scatter.1
  630.6 25.1 all-reduce.2
where the time goes:
time: 666 us
  waiting for transfers between devices  611 us (92%)
  matrix products  33 us (5%)
  between operations  13.8 us (2%)
    reduce_scatter x1, waiting for transfers between devices, per_device(): lax.psum_scatter(lax.dot_general(saved_input, d_pre, (((0,), (0,)), ((),...  331 us
    all_gather x1, waiting for transfers between devices, per_device(): down_whole = lax.all_gather(down_weight, 'fs', axis=1, tiled=True)  137 us
    all_gather x1, waiting for transfers between devices, per_device(): up_whole = lax.all_gather(up_weight, 'fs', axis=0, tiled=True)  117 us
    psum x1, waiting for transfers between devices, per_device(): layer_out = lax.psum(out_part.astype(jnp.bfloat16), 'tp')  25.3 us
  transfers between devices with their start and end apart: 4, of which 4 were waited for; matrix products, arithmetic and copies ran while one was open for 3% of the time, Pallas kernels for 0%

commit v1 on v0

--- a/solution.py
+++ b/solution.py
@@ -8,7 +8,9 @@
     row_count = fwd_input.shape[0]
     stacked = jnp.concatenate([fwd_input, saved_input], axis=0)
     up_whole = lax.all_gather(up_weight, "fs", axis=0, tiled=True)
-    down_whole = lax.all_gather(down_weight, "fs", axis=1, tiled=True)
+    down_whole = jnp.concatenate(
+        lax.all_to_all(jnp.stack([down_weight] * lax.axis_size("fs")), "fs", 0, 0), axis=1
+    )
     pre_both = jnp.dot(stacked, up_whole, preferred_element_type=jnp.float32)
     pre_fwd = pre_both[:row_count]
     pre_bwd = pre_both[row_count:]

time: 666 us -> 687 us (1.032)
  starting transfers between devices: 0.16 us -> 8.65 us
  waiting for transfers between devices: 611 us -> 618 us
    all_gather x1 -> x0, waiting for transfers between devices: 137 us -> none  [per_device(): down_whole = lax.all_gather(down_weight, 'fs', axis=1, tiled=True)]
    all_gather x1, waiting for transfers between devices: 117 us -> 243 us  [per_device(): up_whole = lax.all_gather(up_weight, 'fs', axis=0, tiled=True)]
    reduce_scatter x1, waiting for transfers between devices: 331 us -> 348 us  [per_device(): lax.psum_scatter(lax.dot_general(saved_input, d_pre, (((0,), (0,)), ((),...]
    all_to_all x0 -> x1, starting transfers between devices: none -> 8.52 us  [per_device(): lax.all_to_all(jnp.stack([down_weight] * lax.axis_size('fs')), 'fs', 0, 0)]
  transfers between devices with their start and end apart: 4 -> 4, of which waited for: 4 -> 3; matrix products, arithmetic and copies ran while one was open for 3% -> 4% of each run, Pallas kernels for 0% -> 0%
where the time goes in v1:
time: 687 us
  waiting for transfers between devices  618 us (90%)
  matrix products  32.9 us (5%)
  between operations  13.8 us (2%)
  local copies, waits for them, and re-layouts  12.2 us (2%)
  starting transfers between devices  8.65 us (1%)
    reduce_scatter x1, waiting for transfers between devices, per_device(): lax.psum_scatter(lax.dot_general(saved_input, d_pre, (((0,), (0,)), ((),...  348 us
    all_gather x1, waiting for transfers between devices, per_device(): up_whole = lax.all_gather(up_weight, 'fs', axis=0, tiled=True)  243 us
    psum x1, waiting for transfers between devices, per_device(): layer_out = lax.psum(out_part.astype(jnp.bfloat16), 'tp')  25.5 us
  transfers between devices with their start and end apart: 4, of which 3 were waited for; matrix products, arithmetic and copies ran while one was open for 4% of the time, Pallas kernels for 0%

profile of v1, /device:TPU:0, one launch (start us, length us, event | category | flops | bytes accessed | tf_op | source)
XLA Modules:
  0.0 686.6 jit_solution(3622102171779442758)
XLA Ops:
  7.2 0.0 copy-start
  7.2 0.0 all-gather.2.cloned.1.call-start
  7.2 0.7 all-gather.2.cloned.1.call-update
  7.9 1.2 copy.11
  9.2 4.3 stack.2
  13.5 0.0 copy-start.1
  13.5 8.5 %all-to-all-start = ((bf16[16,2048,128]{1,2,0:T(8,128)(2,1)}), bf16[16,2048,128]{1,2,0:T(8,128)(2,1)}, u32[]{:S(2)}, u32[]{:S(2)}) async-start(bf16[16,2048,128]{1,2,0:T(8,128)(2,1)} %stack.2), calls=%async_computation | async-start | bytes 16777216 | tf_op jit(solution)/shard_map/all_to_all | solution.py:12
  22.0 0.0 reduce-scatter.2.cloned.1.call-start
  22.1 243.3 %all-gather.2.cloned.1.call-done = bf16[2048,2048]{1,0:T(8,128)(2,1)} async-done(((bf16[128,2048]{1,0:T(8,128)(2,1)}), bf16[2048,2048]{1,0:T(8,128)(2,1)}) %all-gather.2.cloned.1.call-update) | async-done | bytes 8388624 | tf_op jit(solution)/shard_map/all_gather | solution.py:10
  265.4 0.0 copy-done.1
  265.4 5.9 fusion.4
  271.3 0.0 all-to-all-done
  271.3 0.0 copy-start.2
  271.3 0.0 copy-done
  271.3 4.8 fusion.1
  276.1 0.0 copy-done.2
  276.1 8.1 %convolution_bitcast_fusion = f32[2048,2048]{0,1:T(8,128)} fusion(bf16[128,2048]{1,0:T(8,128)(2,1)S(1)} %fusion.1, bf16[128,2048]{1,0:T(8,128)(2,1)S(1)} %copy-done.2), kind=kOutput, calls=%fused_computation | convolution fusion | flops 1073741824 | bytes 17825792 | tf_op jit(solution)/shard_map/dot_general | solution.py:30
  284.2 0.0 reduce-scatter.2.cloned.1.call-update
  284.2 0.0 all-reduce.3.cloned.1.call-start
  284.3 7.1 %convolution_convert_fusion = bf16[128,2048]{1,0:T(8,128)(2,1)} fusion(bf16[128,2048]{1,0:T(8,128)(2,1)S(1)} %fusion.1, bf16[2048,2048]{1,0:T(8,128)(2,1)} %all-gather.2.cloned.1.call-done), kind=kOutput, calls=%fused_computation.3 | convolution fusion | flops 1074003968 | bytes 9437184 | tf_op jit(solution)/shard_map/dot_general | solution.py:25
  291.3 7.1 %convolution_convert_fusion.1 = bf16[128,2048]{1,0:T(8,128)(2,1)} fusion(bf16[2048,2048]{0,1:T(8,128)(2,1)} %bitcast.1, f32[256,2048]{1,0:T(8,128)S(1)} %fusion.4), kind=kOutput, calls=%fused_computation.4 | convolution fusion | flops 1074790400 | bytes 9961472 | tf_op jit(solution)/shard_map/dot_general | solution.py:19
  298.4 0.0 all-reduce.3.cloned.1.call-update
  298.4 1.6 copy.12
  300.0 348.2 %reduce-scatter.2.cloned.1.call-done = f32[128,2048]{0,1:T(8,128)} async-done(((f32[2048,2048]{0,1:T(8,128)}), f32[128,2048]{0,1:T(8,128)}) %reduce-scatter.2.cloned.1.call-update) | async-done | bytes 1048592 | tf_op jit(solution)/shard_map/reduce_scatter | solution.py:29
  648.2 1.3 multiply_add_fusion
  649.6 1.3 copy.13
  650.9 25.5 %all-reduce.3.cloned.1.call-done = (bf16[128,2048]{1,0:T(8,128)(2,1)}, bf16[128,2048]{1,0:T(8,128)(2,1)}) async-done(((bf16[128,2048]{1,0:T(8,128)(2,1)}, bf16[128,2048]{1,0:T(8,128)(2,1)}), (bf16[128,2048]{1,0:T(8,128)(2,1)}, bf16[128,2048]{1,0:T(8,128)(2,1)})) %all-reduce.3.cloned.1.call-update) | async-done | bytes 1048592 | tf_op jit(solution)/shard_map/psum | solution.py:20
  676.3 1.9 copy.16
  678.2 1.9 copy.17
Async XLA Ops:
  7.2 264.1 %copy-start = (bf16[128,2048]{1,0:T(8,128)(2,1)S(1)}, bf16[128,2048]{1,0:T(8,128)(2,1)}, u32[]{:S(2)}) copy-start(bf16[128,2048]{1,0:T(8,128)(2,1)} %param.8) | copy-start | bytes 1572868
  7.2 258.2 %all-gather.2.cloned.1.call-start = ((), (), s32[]{:S(2)}) async-start(), calls=%async_computation.2 | async-start | bytes 8912896 | tf_op jit(solution)/shard_map/all_gather | solution.py:10
  13.5 251.9 %copy-start.1 = (bf16[128,2048]{1,0:T(8,128)(2,1)S(1)}, bf16[128,2048]{1,0:T(8,128)(2,1)}, u32[]{:S(2)}) copy-start(bf16[128,2048]{1,0:T(8,128)(2,1)} %param.7) | copy-start | bytes 1572868
  13.5 257.8 %all-to-all-start = ((bf16[16,2048,128]{1,2,0:T(8,128)(2,1)}), bf16[16,2048,128]{1,2,0:T(8,128)(2,1)}, u32[]{:S(2)}, u32[]{:S(2)}) async-start(bf16[16,2048,128]{1,2,0:T(8,128)(2,1)} %stack.2), calls=%async_computation | async-start | bytes 16777216 | tf_op jit(solution)/shard_map/all_to_all | solution.py:12
  22.0 626.2 %reduce-scatter.2.cloned.1.call-start = ((), (), s32[]{:S(2)}) async-start(), calls=%async_computation.3 | async-start | bytes 17825792 | tf_op jit(solution)/shard_map/reduce_scatter | solution.py:29
  271.3 4.8 copy-start.2
  284.2 392.1 %all-reduce.3.cloned.1.call-start = ((), (), s32[]{:S(2)}) async-start(), calls=%async_computation.4 | async-start | bytes 2097152 | tf_op jit(solution)/shard_map/psum | solution.py:20
Sparse Core Ops, SparseCore 0:
  10.8 254.5 all-gather.1
  284.3 363.8 reduce-scatter.1
  651.2 25.1 all-reduce.2
